TPU v7x, 32 devices: a whole 2x2x4 slice. The times are simulated.
32 devices in a mesh: sp: 32 (over z, y, x, core), tp: 1.
Axes of the slice: x: 2, y: 2, z: 4, core: 2. Of those that a mesh axis runs over, the one named last changes fastest.
Arguments:
- queries: bfloat16 [8192, 1024], P('sp', 'tp'), may hold values from -30 to 30
- keys: bfloat16 [8192, 256], P('sp', 'tp'), may hold values from -30 to 30
- values: bfloat16 [8192, 256], P('sp', 'tp'), may hold values from -20 to 20
- gate_totals: float32 [8192, 16], P('sp', 'tp'), may hold values from -8192 to 0, as said below
- documents: int32 [8192], P('sp'), may hold values from 0 to 1, never falling along the last dimension, each value on 1 to 6144 neighbouring positions
- stream: bfloat16 [8192, 2048], P(('sp', 'tp')), may hold values from -3 to 3
- out_weight: bfloat16 [1024, 2048], replicated, may hold values from -0.1875 to 0.1875
- norm_gain: float32 [2048], replicated, may hold values from 0.1 to 1.9
- routes: int32 [8192, 2], P(('sp', 'tp')), may hold values from 0 to 31, all different within a row; in each aligned block of 256 rows (0 to 255, 256 to 511, ...) at most 32 rows name the same one
- route_weights: float32 [8192, 2], P(('sp', 'tp')), may hold values from 0.2 to 1
- expert_gate: bfloat16 [32, 2048, 1024], P('sp', None, 'tp'), may hold values from -0.125 to 0.125
- expert_up: bfloat16 [32, 2048, 1024], P('sp', None, 'tp'), may hold values from -0.125 to 0.125
- expert_down: bfloat16 [32, 1024, 2048], P('sp', 'tp'), may hold values from -0.1875 to 0.1875
Outputs:
- output: bfloat16 [8192, 2048], P(('sp', 'tp'))
Inputs may be any that keep to these rules, and one draw needn't show every extreme that they name: `gate_totals`: along positions it never rises, for every head. `routes`: in each aligned block of rows held by one device, no expert is named by more than 32 rows.
All inputs are finite; a program needn't handle non-finite values.
Results may differ from a plain program's by a relative error of at most 0.014.
Values may be sent and summed in bfloat16 or wider, within the bound.
A program may use at most 128 MiB of HBM per device.

v0:
```python
import functools
import math

import jax
import jax.numpy as jnp
from jax import lax
from jax.experimental import pallas as pl
from jax.experimental.pallas import tpu as pltpu
from jax.sharding import PartitionSpec as P

QUERY_HEAD_COUNT = 16
KV_HEADS = 4
HD = 64
TOP = 2


EPS = 1e-06
MASKED = -1e30


def make_fold(query_rows, query_gate, key_gate_all, query_docs, first_pos, kv_local, group):
    count = query_rows.shape[0]
    scale = HD ** (-0.5)
    query_blk = query_rows.reshape(count, kv_local, group, HD)
    gate_here = query_gate.T.reshape(kv_local, group, count, 1)
    query_pos = first_pos + jnp.arange(count, dtype=jnp.int32)
    last_pos = first_pos + count - 1
    first_doc = query_docs[0]

    def block_step(carry, block_in):
        running_max, running_sum, carried = carry
        key_block, value_block, doc_block, pos_block = block_in
        width = key_block.shape[0]

        def compute(unused):
            key_heads = key_block.reshape(width, kv_local, HD)
            value_heads = value_block.reshape(width, kv_local, HD)
            gate_keys = lax.dynamic_slice_in_dim(key_gate_all, pos_block[0], width, 0).T.reshape(
                kv_local, group, 1, width
            )
            scores = (
                jnp.einsum(
                    "qkgd,nkd->kgqn", query_blk, key_heads, preferred_element_type=jnp.float32
                )
                * scale
                + gate_here
                - gate_keys
            )
            allowed = (pos_block[None, :] <= query_pos[:, None]) & (
                doc_block[None, :] == query_docs[:, None]
            )
            scores = jnp.where(allowed, scores, MASKED)
            new_max = jnp.maximum(running_max, jnp.max(scores, axis=-1))
            weights = jnp.where(allowed, jnp.exp(scores - new_max[..., None]), 0.0)
            factor = jnp.exp(running_max - new_max)
            new_sum = running_sum * factor + jnp.sum(weights, axis=-1)
            new_carried = carried * factor[..., None] + jnp.einsum(
                "kgqn,nkd->kgqd",
                weights.astype(jnp.bfloat16),
                value_heads,
                preferred_element_type=jnp.float32,
            )
            return (new_max, new_sum, new_carried)

        skipped = (pos_block[0] > last_pos) | (doc_block[width - 1] < first_doc)
        return (lax.cond(skipped, lambda unused: carry, compute, 0), None)

    def fold(carry, piece, start):
        key_piece, value_piece, doc_piece = piece
        length = key_piece.shape[0]
        width = math.gcd(length, 512)
        blocks_count = length // width
        pos_piece = jnp.arange(length, dtype=jnp.int32)
        blocks = (
            key_piece.reshape(blocks_count, width, -1),
            value_piece.reshape(blocks_count, width, -1),
            doc_piece.reshape(blocks_count, width),
            pos_piece.reshape(blocks_count, width),
        )
        carry, unused = lax.scan(block_step, carry, blocks)
        return carry

    initial = (
        jnp.full((kv_local, group, count), MASKED, jnp.float32),
        jnp.zeros((kv_local, group, count), jnp.float32),
        jnp.zeros((kv_local, group, count, HD), jnp.float32),
    )
    return (fold, initial)


def finish(running_sum, carried):
    mixed = carried / running_sum[..., None]
    count = mixed.shape[2]
    return jnp.transpose(mixed, (2, 0, 1, 3)).reshape(count, -1).astype(jnp.bfloat16)


def shards(
    queries,
    keys,
    values,
    gate_totals,
    documents,
    stream,
    out_weight,
    norm_gain,
    routes,
    route_weights,
    expert_gate,
    expert_up,
    expert_down,
):
    tp_count = lax.axis_size("tp")
    sp_count = lax.axis_size("sp")
    tp_index = lax.axis_index("tp")
    sp_index = lax.axis_index("sp")
    group = QUERY_HEAD_COUNT // KV_HEADS
    tok_local = queries.shape[0]
    own_rows = tok_local // tp_count
    first_row = sp_index * tok_local
    query_rows = lax.all_to_all(queries, "tp", split_axis=0, concat_axis=1, tiled=True)
    key_whole, value_whole = (
        lax.all_gather(keys, "tp", axis=1, tiled=True),
        lax.all_gather(values, "tp", axis=1, tiled=True),
    )
    gate_whole = lax.all_gather(gate_totals, "tp", axis=1, tiled=True)
    key_gate_all = lax.all_gather(gate_whole, "sp", axis=0, tiled=True)
    query_gate = lax.dynamic_slice_in_dim(gate_whole, tp_index * own_rows, own_rows, 0)
    query_docs = lax.dynamic_slice_in_dim(documents, tp_index * own_rows, own_rows, 0)
    fold, initial = make_fold(
        query_rows,
        query_gate,
        key_gate_all,
        query_docs,
        first_row + tp_index * own_rows,
        KV_HEADS,
        group,
    )
    running_max, running_sum, carried = fold(
        initial,
        (
            lax.all_gather(key_whole, "sp", axis=0, tiled=True),
            lax.all_gather(value_whole, "sp", axis=0, tiled=True),
            lax.all_gather(documents, "sp", axis=0, tiled=True),
        ),
        jnp.int32(0),
    )
    attended = finish(running_sum, carried)
    hidden = (
        stream.astype(jnp.float32)
        + jnp.dot(attended, out_weight, preferred_element_type=jnp.float32)
    ).astype(jnp.bfloat16)
    hidden_f = hidden.astype(jnp.float32)
    normed = (
        hidden_f
        * lax.rsqrt(jnp.mean(hidden_f * hidden_f, axis=-1, keepdims=True) + EPS)
        * norm_gain
    ).astype(jnp.bfloat16)
    local_experts = expert_gate.shape[0]
    experts_total = local_experts * sp_count
    capacity = max(2, 2 * tok_local * TOP // (tp_count * experts_total))
    flat = routes.reshape(-1)
    hits = (flat[:, None] == jnp.arange(experts_total, dtype=jnp.int32)[None, :]).astype(jnp.int32)
    slot_index = jnp.sum(jnp.cumsum(hits, axis=0) * hits, axis=1) - 1
    target = flat * capacity + slot_index
    entry_rows = jnp.repeat(normed, TOP, axis=0)
    outgoing = (
        jnp.zeros((experts_total * capacity, normed.shape[1]), jnp.bfloat16)
        .at[target]
        .set(entry_rows)
    )
    outgoing = outgoing.reshape(experts_total, capacity, -1)
    arrived = lax.all_to_all(outgoing, "sp", split_axis=0, concat_axis=0, tiled=True)
    slots = arrived.shape[1]
    both_halves = lax.all_gather(arrived, "tp", axis=0, tiled=True)
    grouped = both_halves.reshape(tp_count * sp_count, local_experts, slots, -1)
    gate = jnp.einsum("secd,edf->secf", grouped, expert_gate, preferred_element_type=jnp.float32)
    upper = jnp.einsum("secd,edf->secf", grouped, expert_up, preferred_element_type=jnp.float32)
    inner = (jax.nn.silu(gate) * upper).astype(jnp.bfloat16)
    partial_value = jnp.einsum(
        "secf,efd->secd", inner, expert_down, preferred_element_type=jnp.float32
    )
    partial_value = lax.optimization_barrier(partial_value.astype(jnp.bfloat16)).astype(jnp.float32)
    summed = lax.psum_scatter(
        partial_value.reshape(tp_count * sp_count * local_experts, slots, -1).astype(jnp.bfloat16),
        "tp",
        scatter_dimension=0,
        tiled=True,
    )
    returned = lax.all_to_all(summed, "sp", split_axis=0, concat_axis=0, tiled=True)
    answers = returned.reshape(experts_total * capacity, -1)[target].reshape(own_rows, TOP, -1)
    routed = jnp.sum(route_weights[..., None] * answers.astype(jnp.float32), axis=1)
    return (hidden_f + routed).astype(jnp.bfloat16)


def attend_kernel(sub, span, boundary_ref, query_ref, kv_ref, gate_ref, out_ref):
    tile = pl.program_id(0)
    stripes = kv_ref.shape[0]
    stripe = lax.rem(lax.axis_index("sp"), stripes)
    blocks = query_ref.shape[0]
    block = span // blocks
    group = QUERY_HEAD_COUNT // KV_HEADS
    rows = blocks * sub
    boundary = boundary_ref[0]
    first = tile * span
    heads = []
    zeros = jnp.zeros((rows, HD), jnp.bfloat16)
    query = query_ref[...].reshape(rows, group * HD) * jnp.bfloat16(HD ** (-0.5))
    for head in range(group):
        heads.append(jnp.concatenate([query[:, head * HD:(head + 1) * HD], zeros], axis=1))
    row = lax.broadcasted_iota(jnp.int32, (rows, 1), 0)
    query_pos = first + (row // sub) * block + stripe * sub + lax.rem(row, sub)
    doc_start = jnp.where(query_pos >= boundary, boundary, 0)

    def chunk(index, carry, masked):
        per_z = stripes // blocks
        kv = kv_ref[pl.ds(lax.rem(index, per_z) * blocks, blocks), index // per_z, 0:block, :]
        kv = kv.reshape(span, 2 * HD)
        gates = gate_ref[index]
        origin = gate_ref[tile][:, 0:1]
        bias = origin - gates
        if masked:
            key_pos = index * span + lax.broadcasted_iota(jnp.int32, (1, span), 1)
            allowed = (key_pos <= query_pos) & (key_pos >= doc_start)
        result = []
        for head in range(group):
            top, total, mixed = carry[head]
            score = lax.dot_general(
                heads[head], kv, (((1,), (1,)), ((), ())), preferred_element_type=jnp.float32
            )
            score = score + bias[head:head + 1, :]
            if masked:
                score = jnp.where(allowed, score, MASKED)
            new_top = jnp.maximum(top, jnp.max(score, axis=1, keepdims=True))
            weight = jnp.exp(score - new_top)
            factor = jnp.exp(top - new_top)
            total = total * factor + jnp.sum(weight, axis=1, keepdims=True)
            mixed = mixed * factor + jnp.dot(
                weight.astype(jnp.bfloat16), kv, preferred_element_type=jnp.float32
            )
            result.append((new_top, total, mixed))
        return tuple(result)

    carry = tuple(
        (
            jnp.full((rows, 1), 0.5 * MASKED, jnp.float32),
            jnp.zeros((rows, 1), jnp.float32),
            jnp.zeros((rows, 2 * HD), jnp.float32),
        )
        for unused in range(group)
    )
    low = jnp.where(first >= boundary, boundary // span, 0)
    inside = (boundary > first) & (boundary < first + span)
    clean_low = jnp.where(inside, tile, jnp.where(first >= boundary, (boundary + span - 1) // span, 0))
    clean_low = jnp.minimum(clean_low, tile)
    carry = lax.fori_loop(low, clean_low, lambda i, c: chunk(i, c, True), carry)
    carry = lax.fori_loop(clean_low, tile, lambda i, c: chunk(i, c, False), carry)
    carry = chunk(tile, carry, True)
    parts = [mixed[:, HD:] / total for unused, total, mixed in carry]
    out_ref[...] = jnp.concatenate(parts, axis=1).astype(jnp.bfloat16).reshape(out_ref.shape)


def fast_shards(
    queries,
    keys,
    values,
    gate_totals,
    documents,
    stream,
    out_weight,
    norm_gain,
    routes,
    route_weights,
    expert_gate,
    expert_up,
    expert_down,
):
    sp_count = lax.axis_size("sp")
    group = QUERY_HEAD_COUNT // KV_HEADS
    tok = queries.shape[0]
    stripes = sp_count // KV_HEADS
    sub = tok // stripes
    blocks = 4
    span = blocks * tok
    tiles = sp_count // blocks
    lanes = 2 * HD
    part_a = lax.reduce_precision(gate_totals, 8, 7)
    rest = gate_totals - part_a
    part_b = lax.reduce_precision(rest, 8, 7)
    part_c = rest - part_b
    parts = jnp.stack([part_a, part_b, part_c], axis=0).astype(jnp.bfloat16)
    parts = jnp.transpose(parts.reshape(3, tok, KV_HEADS, group), (2, 0, 3, 1))
    parts = parts.reshape(KV_HEADS, 3 * group, tok)
    docs = jnp.broadcast_to(documents.astype(jnp.bfloat16)[None, None, :], (KV_HEADS, 4, tok))
    extra = jnp.concatenate([parts, docs], axis=1).reshape(KV_HEADS, -1, lanes)
    kv = jnp.concatenate(
        [keys.reshape(tok, KV_HEADS, HD), values.reshape(tok, KV_HEADS, HD)], axis=2
    )
    message = jnp.concatenate([jnp.transpose(kv, (1, 0, 2)), extra], axis=1)
    across = [[g * stripes + j for g in range(KV_HEADS)] for j in range(stripes)]
    within = [[g * stripes + j for j in range(stripes)] for g in range(KV_HEADS)]
    column = lax.all_to_all(
        message, "sp", split_axis=0, concat_axis=0, axis_index_groups=across, tiled=True
    )
    kv_all = lax.all_gather(column, "sp", axis=0, axis_index_groups=within)
    query_send = jnp.transpose(
        queries.reshape(stripes, sub, KV_HEADS, group * HD), (2, 0, 1, 3)
    ).reshape(sp_count, sub, group * HD)
    query_got = lax.all_to_all(query_send, "sp", split_axis=0, concat_axis=0, tiled=True)
    extra_all = jnp.transpose(kv_all[:, :, tok:, :], (1, 0, 2, 3)).reshape(sp_count, 16, tok)
    extra_all = extra_all.astype(jnp.float32)
    boundary = jnp.sum((extra_all[:, 3 * group, :] < 0.5).astype(jnp.int32)).reshape(1)
    gates = extra_all[:, :group] + extra_all[:, group:2 * group] + extra_all[:, 2 * group:3 * group]
    gates = jnp.transpose(gates.reshape(tiles, blocks, group, tok), (0, 2, 1, 3))
    gates = gates.reshape(tiles, group, span)
    mixed = pl.pallas_call(
        functools.partial(attend_kernel, sub, span),
        grid=(tiles,),
        in_specs=[
            pl.BlockSpec(memory_space=pltpu.SMEM),
            pl.BlockSpec((blocks, sub, group * HD), lambda i: (i, 0, 0)),
            pl.BlockSpec(kv_all.shape, lambda i: (0, 0, 0, 0)),
            pl.BlockSpec(gates.shape, lambda i: (0, 0, 0)),
        ],
        out_specs=pl.BlockSpec((blocks, sub, group * HD), lambda i: (i, 0, 0)),
        out_shape=jax.ShapeDtypeStruct((sp_count, sub, group * HD), jnp.bfloat16),
        compiler_params=pltpu.CompilerParams(vmem_limit_bytes=48 * 1024 * 1024),
        name="attend",
    )(boundary, query_got, kv_all, gates)
    back = lax.all_to_all(mixed, "sp", split_axis=0, concat_axis=0, tiled=True)
    attended = jnp.transpose(
        back.reshape(KV_HEADS, stripes, sub, group * HD), (1, 2, 0, 3)
    ).reshape(tok, QUERY_HEAD_COUNT * HD)
    hidden = (
        stream.astype(jnp.float32)
        + jnp.dot(attended, out_weight, preferred_element_type=jnp.float32)
    ).astype(jnp.bfloat16)
    hidden_f = hidden.astype(jnp.float32)
    normed = (
        hidden_f
        * lax.rsqrt(jnp.mean(hidden_f * hidden_f, axis=-1, keepdims=True) + EPS)
        * norm_gain
    ).astype(jnp.bfloat16)
    experts_total = sp_count
    capacity = max(2, 2 * tok * TOP // experts_total)
    slots = experts_total * capacity
    flat = routes.reshape(-1)
    hits = (flat[:, None] == jnp.arange(experts_total, dtype=jnp.int32)[None, :]).astype(jnp.int32)
    slot_index = jnp.sum(jnp.cumsum(hits, axis=0) * hits, axis=1) - 1
    target = (flat * capacity + slot_index).reshape(tok, TOP)
    line = jnp.arange(slots, dtype=jnp.int32)
    placed = sum(
        (line[:, None] == target[:, k][None, :]).astype(jnp.bfloat16) for k in range(TOP)
    )
    outgoing = jnp.dot(placed, normed, preferred_element_type=jnp.float32).astype(jnp.bfloat16)
    arrived = lax.all_to_all(
        outgoing.reshape(experts_total, capacity, -1), "sp", split_axis=0, concat_axis=0, tiled=True
    ).reshape(slots, -1)
    gate = jnp.dot(arrived, expert_gate[0], preferred_element_type=jnp.float32)
    upper = jnp.dot(arrived, expert_up[0], preferred_element_type=jnp.float32)
    inner = (jax.nn.silu(gate) * upper).astype(jnp.bfloat16)
    answer = jnp.dot(inner, expert_down[0], preferred_element_type=jnp.float32).astype(jnp.bfloat16)
    returned = lax.all_to_all(
        answer.reshape(sp_count, capacity, -1), "sp", split_axis=0, concat_axis=0, tiled=True
    ).reshape(slots, -1)
    share = sum(
        jnp.where(line[None, :] == target[:, k][:, None], route_weights[:, k][:, None], 0.0)
        for k in range(TOP)
    )
    share_high = lax.reduce_precision(share, 8, 7)
    share_low = (share - share_high).astype(jnp.bfloat16)
    routed = jnp.dot(
        share_high.astype(jnp.bfloat16), returned, preferred_element_type=jnp.float32
    ) + jnp.dot(share_low, returned, preferred_element_type=jnp.float32)
    return (hidden_f + routed).astype(jnp.bfloat16)


def solution(mesh):
    sp_count, tp_count = mesh.shape["sp"], mesh.shape["tp"]
    fast = tp_count == 1 and sp_count % 32 == 0
    return jax.shard_map(
        fast_shards if fast else shards,
        mesh=mesh,
        in_specs=(
            P("sp", "tp"),
            P("sp", "tp"),
            P("sp", "tp"),
            P("sp", "tp"),
            P("sp"),
            P(("sp", "tp"), None),
            P(),
            P(),
            P(("sp", "tp"), None),
            P(("sp", "tp"), None),
            P("sp", None, "tp"),
            P("sp", None, "tp"),
            P("sp", "tp", None),
        ),
        out_specs=P(("sp", "tp"), None),
        check_vma=False,
    )
```

profile of v0, /device:TPU:0, one launch (start us, length us, event | category | flops | bytes accessed | tf_op | source)
XLA Modules:
  0.0 358.1 jit_solution(14587758942010530801)
XLA Ops:
  6.5 0.0 copy-start.1
  6.5 0.0 copy-start.2
  6.5 0.0 all-gather.3.cloned.1.call-start
  6.5 0.8 reduce-precision_convert_fusion.3
  7.4 0.7 convert_element_type.60
  8.2 0.1 copy.69
  8.3 1.0 copy.63
  9.3 1.0 copy.64
  10.4 0.2 copy.70
  10.7 15.8 %all_to_all.25 = bf16[4,288,128]{2,1,0:T(8,128)(2,1)} all-to-all(bf16[4,288,128]{2,1,0:T(8,128)(2,1)S(1)} %copy.70), channel_id=1, replica_groups={{0,8,16,24},{1,9,17,25},{2,10,18,26},{3,11,19,27},{4,12,20,28},{5,13,21..., dimensions={0} | all-to-all | bytes 589824 | tf_op jit(solution)/shard_map/all_to_all | solution.py:301
  26.5 0.0 all-gather.3.cloned.1.call-update
  26.5 0.0 copy-done.1
  26.5 0.4 reshape.100
  26.9 0.9 copy.72
  27.8 3.7 %all-to-all-start.1 = ((bf16[32,32,256]{2,1,0:T(8,128)(2,1)}), bf16[32,32,256]{2,1,0:T(8,128)(2,1)S(1)}, u32[]{:S(2)}, u32[]{:S(2)}) async-start(bf16[32,32,256]{2,1,0:T(8,128)(2,1)} %bitcast.9), calls=%async_computation.1 | async-start | bytes 1048576 | tf_op jit(solution)/shard_map/all_to_all | solution.py:308
  31.5 0.0 copy-done.2
  31.5 0.1 copy.74
  31.7 0.1 eq.86
  31.8 26.2 %all-gather.3.cloned.1.call-done = bf16[32,288,128]{2,1,0:T(8,128)(2,1)} async-done(((bf16[4,288,128]{2,1,0:T(8,128)(2,1)}), bf16[32,288,128]{2,1,0:T(8,128)(2,1)}) %all-gather.3.cloned.1.call-update) | async-done | bytes 2359312 | tf_op jit(solution)/shard_map/all_gather | solution.py:304
  58.0 0.0 copy-start
  58.0 1.2 convert_bitcast_fusion
  59.3 0.9 reshape.111
  60.2 1.6 fusion.42
  61.8 1.2 slice_add_fusion
  63.0 0.0 all-to-all-done.1.query_ref
  63.0 0.0 copy-done
  63.0 43.8 %attend.1 = bf16[32,32,256]{2,1,0:T(8,128)(2,1)} custom-call(s32[1]{0:T(128)} %bitcast.7.boundary_ref, bf16[32,32,256]{2,1,0:T(8,128)(2,1)S(1)} %all-to-all-done.1.query_ref, bf16[8,4,288,128]{3,2,1,0:T(8,128)(2,1)S(1)} %bitcast.76, f32[8,4,1024]{2,1,0:T(4,128)S(1)} %bitcast.77), custom_call_target="tpu_custom_call" | custom-call | tf_op jit(solution)/shard_map/attend/pallas_call | solution.py:315
  106.9 4.6 %all-to-all-start.2 = ((bf16[32,32,256]{2,1,0:T(8,128)(2,1)}), bf16[32,32,256]{2,1,0:T(8,128)(2,1)S(1)}, u32[]{:S(2)}, u32[]{:S(2)}) async-start(bf16[32,32,256]{2,1,0:T(8,128)(2,1)} %attend.1), calls=%async_computation.2 | async-start | bytes 1048576 | tf_op jit(solution)/shard_map/all_to_all | solution.py:329
  111.5 0.1 eq.82
  111.6 1.2 reduce-window.6
  112.8 0.2 slice_reduce_fusion
  113.1 0.1 fusion.40
  113.2 0.1 sub.18
  113.3 0.1 copy.77
  113.4 13.7 %all-to-all-done.2 = bf16[32,32,256]{2,1,0:T(8,128)(2,1)S(1)} async-done(((bf16[32,32,256]{2,1,0:T(8,128)(2,1)}), bf16[32,32,256]{2,1,0:T(8,128)(2,1)S(1)}, u32[]{:S(2)}, u32[]{:S(2)}) %all-to-all-start.2) | async-done | bytes 524320 | tf_op jit(solution)/shard_map/all_to_all | solution.py:329
  127.1 0.4 copy.73
  127.5 0.1 copy.79
  127.6 0.0 copy-start.3
  127.6 3.9 %fusion.13 = (f32[256]{0:T(256)S(1)}, bf16[256,2048]{1,0:T(8,128)(2,1)S(1)}) fusion(bf16[256,1024]{1,0:T(8,128)(2,1)S(1)} %bitcast.84, bf16[1024,2048]{1,0:T(8,128)(2,1)} %param.19, bf16[256,2048]{1,0:T(8,128)(2,1)} %param.18), kind=kOutput, calls=%fused_computation.16 | convolution fusion | flops 1076887296 | bytes 6816768 | tf_op jit(solution)/shard_map/dot_general | solution.py:335
  131.5 0.0 copy-done.3
  131.5 1.4 convolution_convert_fusion
  133.0 0.0 copy-start.5
  133.0 96.4 %all_to_all.26 = bf16[32,32,2048]{2,1,0:T(8,128)(2,1)S(1)} all-to-all(bf16[32,32,2048]{2,1,0:T(8,128)(2,1)S(1)} %bitcast.78), channel_id=1, replica_groups=mesh['sp'=32,'tp'=1] {'sp'}, dimensions={0} | all-to-all | bytes 8388608 | tf_op jit(solution)/shard_map/all_to_all | solution.py:355
  229.4 0.0 copy-done.5
  229.4 0.0 copy-start.6
  229.4 4.5 %fusion.2 = f32[1024,1024]{1,0:T(8,128)S(1)} fusion(bf16[1024,2048]{1,0:T(8,128)(2,1)S(1)} %bitcast.80, bf16[1,2048,1024]{2,1,0:T(8,128)(2,1)S(1)} %copy-done.5), kind=kOutput, calls=%fused_computation.2 | convolution fusion | flops 4294967296 | bytes 12582912 | tf_op jit(solution)/shard_map/dot_general | solution.py:359
  233.9 0.0 copy-done.6
  233.9 0.0 copy-start.7
  233.9 5.4 %multiply_convert_fusion = bf16[1024,1024]{1,0:T(8,128)(2,1)S(1)} fusion(f32[1024,1024]{1,0:T(8,128)S(1)} %fusion.2, bf16[1024,2048]{1,0:T(8,128)(2,1)S(1)} %bitcast.81, bf16[1,2048,1024]{2,1,0:T(8,128)(2,1)S(1)} %copy-done.6), kind=kOutput, calls=%fused_computation.6 | convolution fusion | flops 4301258752 | bytes 14680064 | tf_op jit(solution)/shard_map/dot_general | solution.py:358
  239.3 0.0 copy-done.7
  239.3 6.1 %fusion.6 = bf16[1024,2048]{1,0:T(8,128)(2,1)} fusion(bf16[1024,1024]{1,0:T(8,128)(2,1)S(1)} %multiply_convert_fusion, bf16[1,1024,2048]{2,1,0:T(8,128)(2,1)S(1)} %copy-done.7), kind=kOutput, calls=%fused_computation.8 | convolution fusion | flops 4297064448 | bytes 10485760 | tf_op jit(solution)/shard_map/dot_general | solution.py:361
  245.4 0.0 copy-start.4
  245.4 3.8 %all-to-all-start.4 = ((bf16[32,32,2048]{2,1,0:T(8,128)(2,1)}), bf16[32,32,2048]{2,1,0:T(8,128)(2,1)}, u32[]{:S(2)}, u32[]{:S(2)}) async-start(bf16[32,32,2048]{2,1,0:T(8,128)(2,1)} %bitcast.79), calls=%async_computation.4 | async-start | bytes 8388608 | tf_op jit(solution)/shard_map/all_to_all | solution.py:362
  249.2 0.0 copy-done.4
  249.2 93.7 %all-to-all-done.4 = bf16[32,32,2048]{2,1,0:T(8,128)(2,1)} async-done(((bf16[32,32,2048]{2,1,0:T(8,128)(2,1)}), bf16[32,32,2048]{2,1,0:T(8,128)(2,1)}, u32[]{:S(2)}, u32[]{:S(2)}) %all-to-all-start.4) | async-done | bytes 4194336 | tf_op jit(solution)/shard_map/all_to_all | solution.py:362
  342.9 3.6 %fusion.23 = f32[256,2048]{1,0:T(8,128)S(1)} fusion(bf16[1024,2048]{1,0:T(8,128)(2,1)} %bitcast.26, f32[256]{0:T(256)S(1)} %bitcast.96, s32[256]{0:T(256)S(1)} %bitcast.92, f32[256]{0:T(256)S(1)} %bitcast.94, s32[256]{0:T(256)S(1)} %bitcast.89), kind=kOutput, calls=%fused_computation.31 | convolution fusion | flops 1075576832 | bytes 6295552 | tf_op jit(solution)/shard_map/dot_general | solution.py:371
  346.5 4.7 %fusion.11 = bf16[256,2048]{1,0:T(8,128)(2,1)} fusion(f32[256,2048]{1,0:T(8,128)S(1)} %fusion.23, bf16[1024,2048]{1,0:T(8,128)(2,1)} %bitcast.26, bf16[256,2048]{1,0:T(8,128)(2,1)S(1)} %get-tuple-element.13, f32[256]{0:T(256)S(1)} %bitcast.97, s32[256]{0:T(256)S(1)} %bitcast.93, f32[256]{0:T(256)S(1)} %bitcast.95, s32[256]{0:T(256)S(1)} %bitcast.90), kind=kOutput, calls=%fused_computation.14 | convolution fusion | flops 1077936128 | bytes 8392704 | tf_op jit(solution)/shard_map/dot_general | solution.py:373
  (22 shorter events, 0.3 us)
Async XLA Ops:
  6.5 20.0 %copy-start.1 = (bf16[256,1024]{1,0:T(8,128)(2,1)S(1)}, bf16[256,1024]{1,0:T(8,128)(2,1)}, u32[]{:S(2)}) copy-start(bf16[256,1024]{1,0:T(8,128)(2,1)} %param.13) | copy-start | bytes 1572868
  6.5 25.0 %copy-start.2 = (s32[256,2]{0,1:T(2,128)S(1)}, s32[256,2]{0,1:T(2,128)}, u32[]{:S(2)}) copy-start(s32[256,2]{0,1:T(2,128)} %param.21) | copy-start | bytes 6148
  6.5 51.5 %all-gather.3.cloned.1.call-start = ((), (), s32[]{:S(2)}) async-start(), calls=%async_computation.5 | async-start | bytes 2654208 | tf_op jit(solution)/shard_map/all_gather | solution.py:304
  27.8 35.2 %all-to-all-start.1 = ((bf16[32,32,256]{2,1,0:T(8,128)(2,1)}), bf16[32,32,256]{2,1,0:T(8,128)(2,1)S(1)}, u32[]{:S(2)}, u32[]{:S(2)}) async-start(bf16[32,32,256]{2,1,0:T(8,128)(2,1)} %bitcast.9), calls=%async_computation.1 | async-start | bytes 1048576 | tf_op jit(solution)/shard_map/all_to_all | solution.py:308
  58.0 5.0 %copy-start = (bf16[32,288,128]{2,1,0:T(8,128)(2,1)S(1)}, bf16[32,288,128]{2,1,0:T(8,128)(2,1)}, u32[]{:S(2)}) copy-start(bf16[32,288,128]{2,1,0:T(8,128)(2,1)} %all-gather.3.cloned.1.call-done) | copy-start | bytes 7077892
  106.9 20.2 %all-to-all-start.2 = ((bf16[32,32,256]{2,1,0:T(8,128)(2,1)}), bf16[32,32,256]{2,1,0:T(8,128)(2,1)S(1)}, u32[]{:S(2)}, u32[]{:S(2)}) async-start(bf16[32,32,256]{2,1,0:T(8,128)(2,1)} %attend.1), calls=%async_computation.2 | async-start | bytes 1048576 | tf_op jit(solution)/shard_map/all_to_all | solution.py:329
  127.6 3.9 %copy-start.3 = (f32[2048]{0:T(1024)S(1)}, f32[2048]{0:T(1024)}, u32[]{:S(2)}) copy-start(f32[2048]{0:T(1024)} %param.20) | copy-start | bytes 24580
  133.0 96.4 %copy-start.5 = (bf16[1,2048,1024]{2,1,0:T(8,128)(2,1)S(1)}, bf16[1,2048,1024]{2,1,0:T(8,128)(2,1)}, u32[]{:S(2)}) copy-start(bf16[1,2048,1024]{2,1,0:T(8,128)(2,1)} %param.24) | copy-start | bytes 12582916
  229.4 4.5 %copy-start.6 = (bf16[1,2048,1024]{2,1,0:T(8,128)(2,1)S(1)}, bf16[1,2048,1024]{2,1,0:T(8,128)(2,1)}, u32[]{:S(2)}) copy-start(bf16[1,2048,1024]{2,1,0:T(8,128)(2,1)} %param.23) | copy-start | bytes 12582916
  233.9 5.4 %copy-start.7 = (bf16[1,1024,2048]{2,1,0:T(8,128)(2,1)S(1)}, bf16[1,1024,2048]{2,1,0:T(8,128)(2,1)}, u32[]{:S(2)}) copy-start(bf16[1,1024,2048]{2,1,0:T(8,128)(2,1)} %param.25) | copy-start | bytes 12582916
  245.4 3.8 %copy-start.4 = (f32[256,2]{0,1:T(2,128)S(1)}, f32[256,2]{0,1:T(2,128)}, u32[]{:S(2)}) copy-start(f32[256,2]{0,1:T(2,128)} %param.22) | copy-start | bytes 6148
  245.4 97.5 %all-to-all-start.4 = ((bf16[32,32,2048]{2,1,0:T(8,128)(2,1)}), bf16[32,32,2048]{2,1,0:T(8,128)(2,1)}, u32[]{:S(2)}, u32[]{:S(2)}) async-start(bf16[32,32,2048]{2,1,0:T(8,128)(2,1)} %bitcast.79), calls=%async_computation.4 | async-start | bytes 8388608 | tf_op jit(solution)/shard_map/all_to_all | solution.py:362
Sparse Core Ops, SparseCore 0:
  26.7 31.3 all-gather.2
where the time goes:
time: 359 us; the launch traced here: 358 us
  waiting for transfers between devices  134 us (37%)
  blocking collectives  112 us (31%)
  Pallas kernels  43.8 us (12%)
  matrix products  29.6 us (8%)
  between operations  13.7 us (4%)
  starting transfers between devices  12.1 us (3%)
  other arithmetic  6.87 us (2%)
  local copies, waits for them, and re-layouts  6.11 us (2%)
    all_to_all x1, blocking collectives, fast_shards(): lax.all_to_all(outgoing.reshape(experts_total, capacity, -1), 'sp', split...  96.4 us
    all_to_all x1, waiting for transfers between devices, fast_shards(): lax.all_to_all(answer.reshape(sp_count, capacity, -1), 'sp', split_axis=0...  93.7 us
    pallas_call x1, Pallas kernels, fast_shards(): pl.pallas_call(functools.partial(attend_kernel, sub, span), grid=(tiles,)...  43.8 us
    all_gather x1, waiting for transfers between devices, fast_shards(): kv_all = lax.all_gather(column, 'sp', axis=0, axis_index_groups=within)  26.2 us
    all_to_all x1, blocking collectives, fast_shards(): lax.all_to_all(message, 'sp', split_axis=0, concat_axis=0, axis_index_gro...  15.8 us
    all_to_all x1, waiting for transfers between devices, fast_shards(): back = lax.all_to_all(mixed, 'sp', split_axis=0, concat_axis=0, tiled=True)  13.7 us
  transfers between devices with their start and end apart: 4, of which 3 were waited for; matrix products, arithmetic and copies ran while one was open for 2% of the time, Pallas kernels for 0%

commit v1 on v0

--- a/solution.py
+++ b/solution.py
@@ -192,7 +192,7 @@
     return (hidden_f + routed).astype(jnp.bfloat16)
 
 
-def attend_kernel(sub, span, boundary_ref, query_ref, kv_ref, gate_ref, out_ref):
+def attend_kernel(sub, span, width, boundary_ref, query_ref, kv_ref, gate_ref, out_ref):
     tile = pl.program_id(0)
     stripes = kv_ref.shape[0]
     stripe = lax.rem(lax.axis_index("sp"), stripes)
@@ -202,60 +202,69 @@
     rows = blocks * sub
     boundary = boundary_ref[0]
     first = tile * span
-    heads = []
+    per_tile = span // width
+    taken = width // block
     zeros = jnp.zeros((rows, HD), jnp.bfloat16)
     query = query_ref[...].reshape(rows, group * HD) * jnp.bfloat16(HD ** (-0.5))
-    for head in range(group):
-        heads.append(jnp.concatenate([query[:, head * HD:(head + 1) * HD], zeros], axis=1))
+    stacked = jnp.concatenate(
+        [
+            jnp.concatenate([query[:, head * HD:(head + 1) * HD], zeros], axis=1)
+            for head in range(group)
+        ],
+        axis=0,
+    )
     row = lax.broadcasted_iota(jnp.int32, (rows, 1), 0)
     query_pos = first + (row // sub) * block + stripe * sub + lax.rem(row, sub)
     doc_start = jnp.where(query_pos >= boundary, boundary, 0)
+    origin = gate_ref[tile * per_tile][:, :, 0:1]
+    lane = lax.broadcasted_iota(jnp.int32, (width, 2 * HD), 1)
 
     def chunk(index, carry, masked):
-        per_z = stripes // blocks
-        kv = kv_ref[pl.ds(lax.rem(index, per_z) * blocks, blocks), index // per_z, 0:block, :]
-        kv = kv.reshape(span, 2 * HD)
-        gates = gate_ref[index]
-        origin = gate_ref[tile][:, 0:1]
-        bias = origin - gates
+        per_z = stripes // taken
+        kv = kv_ref[pl.ds(lax.rem(index, per_z) * taken, taken), index // per_z, 0:block, :]
+        kv = kv.reshape(width, 2 * HD)
+        bias = origin - gate_ref[index]
         if masked:
-            key_pos = index * span + lax.broadcasted_iota(jnp.int32, (1, span), 1)
+            key_pos = index * width + lax.broadcasted_iota(jnp.int32, (1, width), 1)
             allowed = (key_pos <= query_pos) & (key_pos >= doc_start)
-        result = []
+        scores = lax.dot_general(
+            stacked, kv, (((1,), (1,)), ((), ())), preferred_element_type=jnp.float32
+        )
+        tops, mixed = carry
+        new_tops, factors, weights = [], [], []
         for head in range(group):
-            top, total, mixed = carry[head]
-            score = lax.dot_general(
-                heads[head], kv, (((1,), (1,)), ((), ())), preferred_element_type=jnp.float32
-            )
-            score = score + bias[head:head + 1, :]
+            score = scores[head * rows:(head + 1) * rows] + bias[head]
             if masked:
                 score = jnp.where(allowed, score, MASKED)
-            new_top = jnp.maximum(top, jnp.max(score, axis=1, keepdims=True))
+            new_top = jnp.maximum(tops[head], jnp.max(score, axis=1, keepdims=True))
             weight = jnp.exp(score - new_top)
-            factor = jnp.exp(top - new_top)
-            total = total * factor + jnp.sum(weight, axis=1, keepdims=True)
-            mixed = mixed * factor + jnp.dot(
-                weight.astype(jnp.bfloat16), kv, preferred_element_type=jnp.float32
-            )
-            result.append((new_top, total, mixed))
-        return tuple(result)
-
-    carry = tuple(
-        (
-            jnp.full((rows, 1), 0.5 * MASKED, jnp.float32),
-            jnp.zeros((rows, 1), jnp.float32),
-            jnp.zeros((rows, 2 * HD), jnp.float32),
+            factor = jnp.exp(tops[head] - new_top)
+            new_tops.append(new_top)
+            factors.append(factor)
+            weights.append(weight.astype(jnp.bfloat16))
+        mixed = mixed * jnp.concatenate(factors, axis=0) + jnp.dot(
+            jnp.concatenate(weights, axis=0),
+            jnp.where(lane < HD, jnp.bfloat16(1), kv),
+            preferred_element_type=jnp.float32,
         )
-        for unused in range(group)
-    )
-    low = jnp.where(first >= boundary, boundary // span, 0)
+        return (tuple(new_tops), mixed)
+
+    carry = (
+        tuple(jnp.full((rows, 1), 0.5 * MASKED, jnp.float32) for unused in range(group)),
+        jnp.zeros((group * rows, 2 * HD), jnp.float32),
+    )
+    own = tile * per_tile
     inside = (boundary > first) & (boundary < first + span)
-    clean_low = jnp.where(inside, tile, jnp.where(first >= boundary, (boundary + span - 1) // span, 0))
-    clean_low = jnp.minimum(clean_low, tile)
+    second = first >= boundary
+    low = jnp.where(second, boundary // width, 0)
+    clean_low = jnp.where(inside, own, jnp.where(second, (boundary + width - 1) // width, 0))
+    clean_low = jnp.minimum(clean_low, own)
     carry = lax.fori_loop(low, clean_low, lambda i, c: chunk(i, c, True), carry)
-    carry = lax.fori_loop(clean_low, tile, lambda i, c: chunk(i, c, False), carry)
-    carry = chunk(tile, carry, True)
-    parts = [mixed[:, HD:] / total for unused, total, mixed in carry]
+    carry = lax.fori_loop(clean_low, own, lambda i, c: chunk(i, c, False), carry)
+    carry = lax.fori_loop(own, own + per_tile, lambda i, c: chunk(i, c, True), carry)
+    unused, mixed = carry
+    ratio = mixed[:, HD:] / mixed[:, :HD]
+    parts = [ratio[head * rows:(head + 1) * rows] for head in range(group)]
     out_ref[...] = jnp.concatenate(parts, axis=1).astype(jnp.bfloat16).reshape(out_ref.shape)
 
 
@@ -281,6 +290,7 @@
     sub = tok // stripes
     blocks = 4
     span = blocks * tok
+    width = min(span, 1024)
     tiles = sp_count // blocks
     lanes = 2 * HD
     part_a = lax.reduce_precision(gate_totals, 8, 7)
@@ -301,7 +311,14 @@
     column = lax.all_to_all(
         message, "sp", split_axis=0, concat_axis=0, axis_index_groups=across, tiled=True
     )
-    kv_all = lax.all_gather(column, "sp", axis=0, axis_index_groups=within)
+    kv_all = lax.all_to_all(
+        jnp.broadcast_to(column[None], (stripes,) + column.shape),
+        "sp",
+        split_axis=0,
+        concat_axis=0,
+        axis_index_groups=within,
+        tiled=True,
+    )
     query_send = jnp.transpose(
         queries.reshape(stripes, sub, KV_HEADS, group * HD), (2, 0, 1, 3)
     ).reshape(sp_count, sub, group * HD)
@@ -311,15 +328,16 @@
     boundary = jnp.sum((extra_all[:, 3 * group, :] < 0.5).astype(jnp.int32)).reshape(1)
     gates = extra_all[:, :group] + extra_all[:, group:2 * group] + extra_all[:, 2 * group:3 * group]
     gates = jnp.transpose(gates.reshape(tiles, blocks, group, tok), (0, 2, 1, 3))
-    gates = gates.reshape(tiles, group, span)
+    gates = jnp.transpose(gates.reshape(tiles, group, span // width, 1, width), (0, 2, 1, 3, 4))
+    gates = gates.reshape(-1, group, 1, width)
     mixed = pl.pallas_call(
-        functools.partial(attend_kernel, sub, span),
+        functools.partial(attend_kernel, sub, span, width),
         grid=(tiles,),
         in_specs=[
             pl.BlockSpec(memory_space=pltpu.SMEM),
             pl.BlockSpec((blocks, sub, group * HD), lambda i: (i, 0, 0)),
             pl.BlockSpec(kv_all.shape, lambda i: (0, 0, 0, 0)),
-            pl.BlockSpec(gates.shape, lambda i: (0, 0, 0)),
+            pl.BlockSpec(gates.shape, lambda i: (0, 0, 0, 0)),
         ],
         out_specs=pl.BlockSpec((blocks, sub, group * HD), lambda i: (i, 0, 0)),
         out_shape=jax.ShapeDtypeStruct((sp_count, sub, group * HD), jnp.bfloat16),

time: 359 us -> 349 us (0.972)
  between operations: 13.7 us -> 0.33 us
  waiting for transfers between devices: 134 us -> 147 us
  Pallas kernels: 43.8 us -> 33.1 us
    all_to_all x0 -> x1, waiting for transfers between devices: none -> 28.1 us  [fast_shards(): lax.all_to_all(jnp.broadcast_to(column[None], (stripes,) + column.shape),...]
    all_gather x1 -> x0, waiting for transfers between devices: 26.2 us -> none  [fast_shards(): kv_all = lax.all_gather(column, 'sp', axis=0, axis_index_groups=within)]
    all_to_all x1, waiting for transfers between devices: 0.01 us -> 11.2 us  [fast_shards(): lax.all_to_all(query_send, 'sp', split_axis=0, concat_axis=0, tiled=True)]
    pallas_call x1, Pallas kernels: 43.8 us -> 33.1 us  [fast_shards(): pl.pallas_call(functools.partial(attend_kernel, sub, span, width), grid=(...]
    all_to_all x0 -> x1, starting transfers between devices: none -> 3.85 us  [fast_shards(): lax.all_to_all(jnp.broadcast_to(column[None], (stripes,) + column.shape),...]
  transfers between devices with their start and end apart: 4 -> 4, of which waited for: 3 -> 4; matrix products, arithmetic and copies ran while one was open for 2% -> 2% of each run, Pallas kernels for 0% -> 0%
where the time goes in v1:
time: 349 us
  waiting for transfers between devices  147 us (42%)
  blocking collectives  112 us (32%)
  Pallas kernels  33.1 us (9%)
  matrix products  29.6 us (8%)
  starting transfers between devices  13.1 us (4%)
  local copies, waits for them, and re-layouts  8.1 us (2%)
  other arithmetic  5.76 us (2%)
    all_to_all x1, blocking collectives, fast_shards(): lax.all_to_all(outgoing.reshape(experts_total, capacity, -1), 'sp', split...  96.4 us
    all_to_all x1, waiting for transfers between devices, fast_shards(): lax.all_to_all(answer.reshape(sp_count, capacity, -1), 'sp', split_axis=0...  93.7 us
    pallas_call x1, Pallas kernels, fast_shards(): pl.pallas_call(functools.partial(attend_kernel, sub, span, width), grid=(...  33.1 us
    all_to_all x1, waiting for transfers between devices, fast_shards(): lax.all_to_all(jnp.broadcast_to(column[None], (stripes,) + column.shape),...  28.1 us
    all_to_all x1, blocking collectives, fast_shards(): lax.all_to_all(message, 'sp', split_axis=0, concat_axis=0, axis_index_gro...  15.7 us
    all_to_all x1, waiting for transfers between devices, fast_shards(): back = lax.all_to_all(mixed, 'sp', split_axis=0, concat_axis=0, tiled=True)  13.7 us
    all_to_all x1, waiting for transfers between devices, fast_shards(): lax.all_to_all(query_send, 'sp', split_axis=0, concat_axis=0, tiled=True)  11.2 us
  transfers between devices with their start and end apart: 4, of which 4 were waited for; matrix products, arithmetic and copies ran while one was open for 2% of the time, Pallas kernels for 0%

profile of v1, /device:TPU:0, one launch (start us, length us, event | category | flops | bytes accessed | tf_op | source)
XLA Modules:
  0.0 348.9 jit_solution(17490617531177138348)
XLA Ops:
  0.0 0.7 reduce-precision_convert_fusion.3
  0.8 0.7 convert_element_type.60
  1.6 0.1 copy.72
  1.7 1.0 copy.66
  2.7 1.0 copy.67
  3.8 0.0 copy-start
  3.8 0.2 copy.73
  4.1 15.7 %all_to_all.30 = bf16[4,288,128]{2,1,0:T(8,128)(2,1)S(1)} all-to-all(bf16[4,288,128]{2,1,0:T(8,128)(2,1)S(1)} %copy.73), channel_id=1, replica_groups={{0,8,16,24},{1,9,17,25},{2,10,18,26},{3,11,19,27},{4,12,20,28},{5,13,21..., dimensions={0} | all-to-all | bytes 589824 | tf_op jit(solution)/shard_map/all_to_all | solution.py:311
  19.8 1.8 broadcast_in_dim.42
  21.6 0.0 copy-start.1
  21.6 3.9 %all-to-all-start.1 = ((bf16[8,4,288,128]{3,2,1,0:T(8,128)(2,1)}), bf16[8,4,288,128]{3,2,1,0:T(8,128)(2,1)S(1)}, u32[]{:S(2)}, u32[]{:S(2)}) async-start(bf16[8,4,288,128]{3,2,1,0:T(8,128)(2,1)} %broadcast_in_dim.42), calls=%async_computation.1 | async-start | bytes 4718592 | tf_op jit(solution)/shard_map/all_to_all | solution.py:314
  25.4 0.0 copy-done
  25.4 0.4 reshape.98
  25.8 0.9 copy.75
  26.7 28.1 %all-to-all-done.1.kv_ref = bf16[8,4,288,128]{3,2,1,0:T(8,128)(2,1)S(1)} async-done(((bf16[8,4,288,128]{3,2,1,0:T(8,128)(2,1)}), bf16[8,4,288,128]{3,2,1,0:T(8,128)(2,1)S(1)}, u32[]{:S(2)}, u32[]{:S(2)}) %all-to-all-start.1) | async-done | bytes 2359328 | tf_op jit(solution)/shard_map/all_to_all | solution.py:314
  54.9 2.6 all-to-all-start.2
  57.5 0.0 copy-done.1
  57.5 0.1 copy.78
  57.6 0.1 eq.86
  57.8 0.1 convert_bitcast_fusion
  57.9 0.9 reshape.108
  58.8 1.2 slice_add_fusion
  60.0 0.2 reshape_transpose_reshape.3.gate_ref
  60.2 1.7 fusion.42
  61.9 11.2 %all-to-all-done.2.query_ref = bf16[32,32,256]{2,1,0:T(8,128)(2,1)S(1)} async-done(((bf16[32,32,256]{2,1,0:T(8,128)(2,1)}), bf16[32,32,256]{2,1,0:T(8,128)(2,1)S(1)}, u32[]{:S(2)}, u32[]{:S(2)}) %all-to-all-start.2) | async-done | bytes 524320 | tf_op jit(solution)/shard_map/all_to_all | solution.py:325
  73.1 33.1 %attend.1 = bf16[32,32,256]{2,1,0:T(8,128)(2,1)} custom-call(s32[1]{0:T(128)} %bitcast.6.boundary_ref, bf16[32,32,256]{2,1,0:T(8,128)(2,1)S(1)} %all-to-all-done.2.query_ref, bf16[8,4,288,128]{3,2,1,0:T(8,128)(2,1)S(1)} %all-to-all-done.1.kv_ref, f32[8,4,1,1024]{3,2,1,0:T(1,128)S(1)} %reshape_transpose_reshape.3.gate_ref), custom_call_target="tpu_custom_call" | custom-call | tf_op jit(solution)/shard_map/attend/pallas_call | solution.py:333
  106.2 2.9 all-to-all-start.3
  109.1 0.1 eq.82
  109.3 1.2 reduce-window.6
  110.4 0.2 slice_reduce_fusion
  110.7 0.1 fusion.40
  110.8 0.1 sub.18
  111.0 0.1 copy.81
  111.1 13.7 %all-to-all-done.3 = bf16[32,32,256]{2,1,0:T(8,128)(2,1)S(1)} async-done(((bf16[32,32,256]{2,1,0:T(8,128)(2,1)}), bf16[32,32,256]{2,1,0:T(8,128)(2,1)S(1)}, u32[]{:S(2)}, u32[]{:S(2)}) %all-to-all-start.3) | async-done | bytes 524320 | tf_op jit(solution)/shard_map/all_to_all | solution.py:347
  124.7 0.4 copy.77
  125.1 0.1 copy.83
  125.2 0.0 copy-start.2
  125.3 3.9 %fusion.13 = (f32[256]{0:T(256)S(1)}, bf16[256,2048]{1,0:T(8,128)(2,1)S(1)}) fusion(bf16[256,1024]{1,0:T(8,128)(2,1)S(1)} %bitcast.78, bf16[1024,2048]{1,0:T(8,128)(2,1)} %param.19, bf16[256,2048]{1,0:T(8,128)(2,1)} %param.18), kind=kOutput, calls=%fused_computation.16 | convolution fusion | flops 1076887296 | bytes 6816768 | tf_op jit(solution)/shard_map/dot_general | solution.py:353
  129.2 0.0 copy-done.2
  129.2 1.4 convolution_convert_fusion
  130.6 0.0 copy-start.4
  130.6 96.4 %all_to_all.31 = bf16[32,32,2048]{2,1,0:T(8,128)(2,1)S(1)} all-to-all(bf16[32,32,2048]{2,1,0:T(8,128)(2,1)S(1)} %bitcast.72), channel_id=1, replica_groups=mesh['sp'=32,'tp'=1] {'sp'}, dimensions={0} | all-to-all | bytes 8388608 | tf_op jit(solution)/shard_map/all_to_all | solution.py:373
  227.0 0.0 copy-done.4
  227.0 0.0 copy-start.5
  227.0 4.5 %fusion.2 = f32[1024,1024]{1,0:T(8,128)S(1)} fusion(bf16[1024,2048]{1,0:T(8,128)(2,1)S(1)} %bitcast.74, bf16[1,2048,1024]{2,1,0:T(8,128)(2,1)S(1)} %copy-done.4), kind=kOutput, calls=%fused_computation.2 | convolution fusion | flops 4294967296 | bytes 12582912 | tf_op jit(solution)/shard_map/dot_general | solution.py:377
  231.5 0.0 copy-done.5
  231.5 0.0 copy-start.6
  231.6 5.4 %multiply_convert_fusion = bf16[1024,1024]{1,0:T(8,128)(2,1)S(1)} fusion(f32[1024,1024]{1,0:T(8,128)S(1)} %fusion.2, bf16[1024,2048]{1,0:T(8,128)(2,1)S(1)} %bitcast.75, bf16[1,2048,1024]{2,1,0:T(8,128)(2,1)S(1)} %copy-done.5), kind=kOutput, calls=%fused_computation.6 | convolution fusion | flops 4301258752 | bytes 14680064 | tf_op jit(solution)/shard_map/dot_general | solution.py:376
  236.9 0.0 copy-done.6
  236.9 6.1 %fusion.6 = bf16[1024,2048]{1,0:T(8,128)(2,1)} fusion(bf16[1024,1024]{1,0:T(8,128)(2,1)S(1)} %multiply_convert_fusion, bf16[1,1024,2048]{2,1,0:T(8,128)(2,1)S(1)} %copy-done.6), kind=kOutput, calls=%fused_computation.8 | convolution fusion | flops 4297064448 | bytes 10485760 | tf_op jit(solution)/shard_map/dot_general | solution.py:379
  243.0 0.0 copy-start.3
  243.0 3.8 %all-to-all-start.5 = ((bf16[32,32,2048]{2,1,0:T(8,128)(2,1)}), bf16[32,32,2048]{2,1,0:T(8,128)(2,1)}, u32[]{:S(2)}, u32[]{:S(2)}) async-start(bf16[32,32,2048]{2,1,0:T(8,128)(2,1)} %bitcast.73), calls=%async_computation.5 | async-start | bytes 8388608 | tf_op jit(solution)/shard_map/all_to_all | solution.py:380
  246.8 0.0 copy-done.3
  246.9 93.7 %all-to-all-done.5 = bf16[32,32,2048]{2,1,0:T(8,128)(2,1)} async-done(((bf16[32,32,2048]{2,1,0:T(8,128)(2,1)}), bf16[32,32,2048]{2,1,0:T(8,128)(2,1)}, u32[]{:S(2)}, u32[]{:S(2)}) %all-to-all-start.5) | async-done | bytes 4194336 | tf_op jit(solution)/shard_map/all_to_all | solution.py:380
  340.5 3.6 %fusion.23 = f32[256,2048]{1,0:T(8,128)S(1)} fusion(bf16[1024,2048]{1,0:T(8,128)(2,1)} %bitcast.24, f32[256]{0:T(256)S(1)} %bitcast.91, s32[256]{0:T(256)S(1)} %bitcast.87, f32[256]{0:T(256)S(1)} %bitcast.89, s32[256]{0:T(256)S(1)} %bitcast.84), kind=kOutput, calls=%fused_computation.31 | convolution fusion | flops 1075576832 | bytes 6295552 | tf_op jit(solution)/shard_map/dot_general | solution.py:389
  344.2 4.7 %fusion.11 = bf16[256,2048]{1,0:T(8,128)(2,1)} fusion(f32[256,2048]{1,0:T(8,128)S(1)} %fusion.23, bf16[1024,2048]{1,0:T(8,128)(2,1)} %bitcast.24, bf16[256,2048]{1,0:T(8,128)(2,1)S(1)} %get-tuple-element.13, f32[256]{0:T(256)S(1)} %bitcast.92, s32[256]{0:T(256)S(1)} %bitcast.88, f32[256]{0:T(256)S(1)} %bitcast.90, s32[256]{0:T(256)S(1)} %bitcast.85), kind=kOutput, calls=%fused_computation.14 | convolution fusion | flops 1077936128 | bytes 8392704 | tf_op jit(solution)/shard_map/dot_general | solution.py:391
  (23 shorter events, 0.3 us)
Async XLA Ops:
  3.8 21.6 %copy-start = (bf16[256,1024]{1,0:T(8,128)(2,1)S(1)}, bf16[256,1024]{1,0:T(8,128)(2,1)}, u32[]{:S(2)}) copy-start(bf16[256,1024]{1,0:T(8,128)(2,1)} %param.13) | copy-start | bytes 1572868
  21.6 35.9 %copy-start.1 = (s32[256,2]{0,1:T(2,128)S(1)}, s32[256,2]{0,1:T(2,128)}, u32[]{:S(2)}) copy-start(s32[256,2]{0,1:T(2,128)} %param.21) | copy-start | bytes 6148
  21.6 33.3 %all-to-all-start.1 = ((bf16[8,4,288,128]{3,2,1,0:T(8,128)(2,1)}), bf16[8,4,288,128]{3,2,1,0:T(8,128)(2,1)S(1)}, u32[]{:S(2)}, u32[]{:S(2)}) async-start(bf16[8,4,288,128]{3,2,1,0:T(8,128)(2,1)} %broadcast_in_dim.42), calls=%async_computation.1 | async-start | bytes 4718592 | tf_op jit(solution)/shard_map/all_to_all | solution.py:314
  54.9 18.2 %all-to-all-start.2 = ((bf16[32,32,256]{2,1,0:T(8,128)(2,1)}), bf16[32,32,256]{2,1,0:T(8,128)(2,1)S(1)}, u32[]{:S(2)}, u32[]{:S(2)}) async-start(bf16[32,32,256]{2,1,0:T(8,128)(2,1)} %bitcast.8), calls=%async_computation.2 | async-start | bytes 1048576 | tf_op jit(solution)/shard_map/all_to_all | solution.py:325
  106.2 18.5 %all-to-all-start.3 = ((bf16[32,32,256]{2,1,0:T(8,128)(2,1)}), bf16[32,32,256]{2,1,0:T(8,128)(2,1)S(1)}, u32[]{:S(2)}, u32[]{:S(2)}) async-start(bf16[32,32,256]{2,1,0:T(8,128)(2,1)} %attend.1), calls=%async_computation.3 | async-start | bytes 1048576 | tf_op jit(solution)/shard_map/all_to_all | solution.py:347
  125.2 3.9 %copy-start.2 = (f32[2048]{0:T(1024)S(1)}, f32[2048]{0:T(1024)}, u32[]{:S(2)}) copy-start(f32[2048]{0:T(1024)} %param.20) | copy-start | bytes 24580
  130.6 96.4 %copy-start.4 = (bf16[1,2048,1024]{2,1,0:T(8,128)(2,1)S(1)}, bf16[1,2048,1024]{2,1,0:T(8,128)(2,1)}, u32[]{:S(2)}) copy-start(bf16[1,2048,1024]{2,1,0:T(8,128)(2,1)} %param.24) | copy-start | bytes 12582916
  227.0 4.5 %copy-start.5 = (bf16[1,2048,1024]{2,1,0:T(8,128)(2,1)S(1)}, bf16[1,2048,1024]{2,1,0:T(8,128)(2,1)}, u32[]{:S(2)}) copy-start(bf16[1,2048,1024]{2,1,0:T(8,128)(2,1)} %param.23) | copy-start | bytes 12582916
  231.5 5.4 %copy-start.6 = (bf16[1,1024,2048]{2,1,0:T(8,128)(2,1)S(1)}, bf16[1,1024,2048]{2,1,0:T(8,128)(2,1)}, u32[]{:S(2)}) copy-start(bf16[1,1024,2048]{2,1,0:T(8,128)(2,1)} %param.25) | copy-start | bytes 12582916
  243.0 3.8 %copy-start.3 = (f32[256,2]{0,1:T(2,128)S(1)}, f32[256,2]{0,1:T(2,128)}, u32[]{:S(2)}) copy-start(f32[256,2]{0,1:T(2,128)} %param.22) | copy-start | bytes 6148
  243.0 97.5 %all-to-all-start.5 = ((bf16[32,32,2048]{2,1,0:T(8,128)(2,1)}), bf16[32,32,2048]{2,1,0:T(8,128)(2,1)}, u32[]{:S(2)}, u32[]{:S(2)}) async-start(bf16[32,32,2048]{2,1,0:T(8,128)(2,1)} %bitcast.73), calls=%async_computation.5 | async-start | bytes 8388608 | tf_op jit(solution)/shard_map/all_to_all | solution.py:380
